TPU v7x, 256 devices: a 8x8x2 block of a 8x8x16 slice. The times are simulated.
256 devices in a mesh: grp: 2 (over z), ep: 16 (over y, core), tp: 8 (over x).
Axes of the slice: x: 8, y: 8, z: 2, core: 2. Of those that a mesh axis runs over, the one named last changes fastest.
The devices are a block of a 8x8x16 slice.
Arguments:
- tokens: bfloat16 [32768, 1024], P(('grp', 'ep', 'tp')), parts along dimension 0, may hold values from -6 to 6
- norm_gain: float32 [1024], replicated, may hold values from 0.1 to 1.9
- gate_weight: bfloat16 [16, 1024, 3584], P('ep', None, 'tp'), may hold values from -0.1875 to 0.1875
- up_weight: bfloat16 [16, 1024, 3584], P('ep', None, 'tp'), may hold values from -0.1875 to 0.1875
- down_weight: bfloat16 [16, 3584, 1024], P('ep', 'tp'), may hold values from -0.09375 to 0.09375
- expert_ids: int32 [32768, 2], P(('grp', 'ep')), parts along dimension 0, may hold values from 0 to 15, all different within a row; in each aligned block of 128 rows (0 to 127, 128 to 255, ...) at most 20 rows name the same one
- route_weight: float32 [32768, 2], P(('grp', 'ep')), parts along dimension 0, may hold values from 0.2 to 1
Outputs:
- mixed: bfloat16 [32768, 1024], P(('grp', 'ep', 'tp')), parts along dimension 0
There are 2 independent parts, one for each index of `grp`. A program takes and returns all parts, laid end to end along the dimension named above; an argument that names none is the same for every part. Nothing has to cross between parts.
Inputs may be any that keep to these rules, and one draw needn't show every extreme that they name: `expert_ids`: A token's 2 experts differ. In the rows of one device (128 tokens, aligned blocks) no expert is named more than 20 times, and in every draw some expert is named exactly 20 times in some device's rows.
All inputs are finite; a program needn't handle non-finite values.
Results may differ from a plain program's by a relative error of at most 0.015.
Values may be sent and summed in bfloat16 or wider, within the bound.
No kernel may reach another device: no remote copies, remote signals or barrier semaphores. Data moves between devices by JAX's collectives and lax.ppermute only.
A program may use at most 64 MiB of HBM per device.

v0:
```python
import jax
import jax.numpy as jnp
from jax import lax
from jax.sharding import PartitionSpec as P

TOP_K = 2


def norm_rows(tokens, norm_gain):
    values = tokens.astype(jnp.float32)
    scaled = values * lax.rsqrt(jnp.mean(values * values, axis=-1, keepdims=True) + 1e-06)
    return (scaled * norm_gain).astype(jnp.bfloat16)


def expert_hidden(rows, gate_weight, up_weight):
    gate = jnp.einsum("e...d,edf->e...f", rows, gate_weight, preferred_element_type=jnp.float32)
    upper = jnp.einsum("e...d,edf->e...f", rows, up_weight, preferred_element_type=jnp.float32)
    return (jax.nn.silu(gate) * upper).astype(jnp.bfloat16)


def weigh_pieces(summed, weights):
    piece = lax.optimization_barrier(summed.astype(jnp.bfloat16)).astype(jnp.float32)
    total = piece[:, 0] * weights[:, 0:1]
    total = total + piece[:, 1] * weights[:, 1:2]
    return total.astype(jnp.bfloat16)


def body(tokens, norm_gain, gate_weight, up_weight, down_weight, expert_ids, route_weight):
    tok_rows = tokens.shape[0]
    width = tokens.shape[1]
    local_experts = gate_weight.shape[0]
    inner = gate_weight.shape[2]
    n_tp = lax.axis_size("tp")
    n_ep = lax.axis_size("ep")
    experts = n_ep * local_experts
    most = max(2, tok_rows * TOP_K * 5 // (4 * experts))
    normed = norm_rows(tokens, norm_gain)
    flat_ids = expert_ids.reshape(n_tp, tok_rows * TOP_K)
    onehot = (flat_ids[:, :, None] == jnp.arange(experts, dtype=jnp.int32)[None, None, :]).astype(
        jnp.int32
    )
    before = jnp.cumsum(onehot, axis=1) - onehot
    slots = jnp.sum(before * onehot, axis=-1)
    mine = lax.axis_index("tp")
    own_ids = lax.dynamic_slice_in_dim(flat_ids, mine, 1, 0)[0]
    own_slots = lax.dynamic_slice_in_dim(slots, mine, 1, 0)[0]
    own_index = own_ids * most + own_slots
    sending = (
        jnp.zeros((experts * most, width), jnp.bfloat16)
        .at[own_index]
        .set(jnp.repeat(normed, TOP_K, axis=0))
    )
    arrived = lax.all_to_all(
        sending.reshape(experts, most, width), "ep", split_axis=0, concat_axis=1, tiled=True
    )
    arrived = arrived.reshape(local_experts, n_ep, most, width)
    hidden = expert_hidden(
        lax.all_gather(arrived, "tp", axis=2, tiled=True), gate_weight, up_weight
    )
    hidden = hidden.reshape(local_experts, n_ep * n_tp * most, inner)
    by_source = hidden.reshape(local_experts, n_ep, n_tp, most, inner).transpose(2, 0, 1, 3, 4)
    per_device = local_experts * n_ep * most
    product = jnp.einsum(
        "tlnmf,lfd->tlnmd", by_source, down_weight, preferred_element_type=jnp.float32
    )
    own_sums = lax.psum_scatter(
        product.astype(jnp.bfloat16)
        .astype(jnp.float32)
        .reshape(per_device * lax.axis_size("tp"), width)
        .astype(jnp.bfloat16),
        "tp",
        scatter_dimension=0,
        tiled=True,
    )
    own_pieces = own_sums.reshape(local_experts, n_ep, most, width)
    back = lax.all_to_all(own_pieces, "ep", split_axis=1, concat_axis=0, tiled=True)
    picked = back.reshape(experts * most, width)[own_index].reshape(tok_rows, TOP_K, width)
    own_weights = lax.dynamic_slice_in_dim(route_weight, mine * tok_rows, tok_rows, 0)
    return weigh_pieces(picked.astype(jnp.float32), own_weights)


def solution(mesh):
    placed = (
        P(("grp", "ep", "tp"), None),
        P(),
        P("ep", None, "tp"),
        P("ep", None, "tp"),
        P("ep", "tp", None),
        P(("grp", "ep"), None),
        P(("grp", "ep"), None),
    )
    return jax.shard_map(
        body, mesh=mesh, in_specs=placed, out_specs=P(("grp", "ep", "tp"), None), check_vma=False
    )
```

profile of v0, /device:TPU:513, one launch (start us, length us, event | category | flops | bytes accessed | tf_op | source)
XLA Modules:
  0.0 266.6 jit_solution(17186657709700411521)
XLA Ops:
  6.5 0.0 copy-start
  6.6 0.0 all-gather.3.cloned.1.call-start
  6.6 1.0 copy.18
  7.6 0.0 copy-start.2
  7.6 0.3 eq.26
  7.9 0.3 reshape.112
  8.2 4.6 %reduce-window.6 = s32[8,16,2,128]{3,1,2,0:T(8,128)S(1)} reduce-window(s32[8,16,2,128]{3,1,2,0:T(8,128)S(1)} %fusion.22, s32[]{:T(128)} %constant.6.clone.1), window={size=1x1x1x128 pad=0_0x0_0x0_0x127_0}, to_apply=%region_0.0 | reduce-window | flops 4161536 | bytes 262148 | tf_op jit(solution)/shard_map/reduce-window
  12.7 0.1 slice.26
  12.8 0.2 copy.20
  13.0 0.1 fusion.23
  13.1 1.1 fusion.10
  14.2 1.1 fusion.12
  15.3 0.3 broadcast_in_dim.5
  15.5 0.2 reshape.137
  15.8 0.1 fusion.21
  15.9 1.9 scatter_custom_fusion
  17.8 0.1 reshape.115
  17.9 46.1 %all_to_all.8 = bf16[16,20,1024]{2,1,0:T(8,128)(2,1)S(1)} all-to-all(bf16[16,20,1024]{2,1,0:T(8,128)(2,1)S(1)} %reshape.115), channel_id=1, replica_groups=mesh['grp'=2,'ep'=16,'tp'=8] {'ep'}, dimensions={0} | all-to-all | bytes 1310720 | tf_op jit(solution)/shard_map/all_to_all | solution.py:53
  64.0 1.2 copy.23
  65.2 0.1 all-gather.3.cloned.1.call-update
  65.3 0.0 copy-start.3
  65.3 0.2 reduce-scatter.2.cloned.1.call-start
  65.5 63.5 %all-gather.3.cloned.1.call-done = bf16[16,160,1024]{2,0,1:T(8,128)(2,1)} async-done(((bf16[16,20,1024]{2,0,1:T(8,128)(2,1)}), bf16[16,160,1024]{2,0,1:T(8,128)(2,1)}) %all-gather.3.cloned.1.call-update) | async-done | bytes 5242896 | tf_op jit(solution)/shard_map/all_gather | solution.py:58
  129.0 0.0 copy-done.2
  129.0 0.0 copy-start.1
  129.0 8.7 %fusion = f32[16,160,448]{2,1,0:T(8,128)S(1)} fusion(bf16[16,160,1024]{2,0,1:T(8,128)(2,1)} %all-gather.3.cloned.1.call-done, bf16[1,1024,448]{1,2,0:T(8,128)(2,1)S(1)} %copy-done.2), kind=kOutput, calls=%fused_computation.4 | convolution fusion | flops 2348810240 | bytes 10747904 | tf_op jit(solution)/shard_map/e...d,edf->e...f/dot_general | solution.py:17
  137.7 0.0 copy-done.3
  137.7 0.0 copy-done.1
  137.7 5.0 %multiply_convert_fusion = bf16[16,160,448]{2,1,0:T(8,128)(2,1)S(1)} fusion(f32[16,160,448]{2,1,0:T(8,128)S(1)} %fusion, bf16[16,160,1024]{2,0,1:T(8,128)(2,1)S(1)} %copy-done.1, bf16[1,1024,448]{1,2,0:T(8,128)(2,1)S(1)} %copy-done.3), kind=kOutput, calls=%fused_computation.3 | convolution fusion | flops 2355691520 | bytes 13041664 | tf_op jit(solution)/shard_map/e...d,edf->e...f/dot_general | solution.py:16
  142.7 1.5 copy.26
  144.2 0.0 copy-done
  144.2 6.0 %convert_bitcast_fusion = bf16[8,1,16,20,1024]{4,3,2,0,1:T(8,128)(2,1)} fusion(bf16[8,16,20,448]{3,1,2,0:T(8,128)(2,1)S(1)} %bitcast.74, bf16[1,448,1024]{2,1,0:T(8,128)(2,1)S(1)} %copy-done), kind=kOutput, calls=%fused_computation.2 | convolution fusion | flops 2351431680 | bytes 8454144 | tf_op jit(solution)/shard_map/tlnmf,lfd->tlnmd/dot_general | solution.py:63
  150.2 9.0 %convert_element_type.51 = bf16[2560,1024]{1,0:T(8,128)(2,1)} reshape(bf16[8,1,16,20,1024]{4,3,2,0,1:T(8,128)(2,1)} %convert_bitcast_fusion) | data formatting | bytes 10485760 | tf_op jit(solution)/shard_map/convert_element_type | solution.py:70
  159.2 0.1 reduce-scatter.2.cloned.1.call-update
  159.2 65.5 %reduce-scatter.2.cloned.1.call-done = bf16[320,1024]{1,0:T(8,128)(2,1)} async-done(((bf16[2560,1024]{1,0:T(8,128)(2,1)}), bf16[320,1024]{1,0:T(8,128)(2,1)}) %reduce-scatter.2.cloned.1.call-update) | async-done | bytes 655376 | tf_op jit(solution)/shard_map/reduce_scatter | solution.py:66
  224.8 2.0 reshape.122
  226.8 7.7 %all-to-all-start.1 = ((bf16[1,16,20,1024]{3,2,0,1:T(8,128)(2,1)}), bf16[1,16,20,1024]{3,2,0,1:T(8,128)(2,1)S(1)}, u32[]{:S(2)}, u32[]{:S(2)}) async-start(bf16[1,16,20,1024]{3,2,0,1:T(8,128)(2,1)} %bitcast.17), calls=%async_computation.2 | async-start | bytes 1572864 | tf_op jit(solution)/shard_map/all_to_all | solution.py:76
  234.5 0.7 constant_dynamic-slice_fusion
  235.2 22.0 %all-to-all-done.1 = bf16[1,16,20,1024]{3,2,0,1:T(8,128)(2,1)S(1)} async-done(((bf16[1,16,20,1024]{3,2,0,1:T(8,128)(2,1)}), bf16[1,16,20,1024]{3,2,0,1:T(8,128)(2,1)S(1)}, u32[]{:S(2)}, u32[]{:S(2)}) %all-to-all-start.1) | async-done | bytes 655392 | tf_op jit(solution)/shard_map/all_to_all | solution.py:76
  257.3 0.1 reshape.123
  257.4 1.2 gather_fusion
  258.6 0.2 reshape.124
  258.8 0.1 copy_convert_fusion
  258.9 0.8 fusion.15
  (7 shorter events, 0.1 us)
Async XLA Ops:
  6.5 137.7 %copy-start = (bf16[1,448,1024]{2,1,0:T(8,128)(2,1)S(1)}, bf16[1,448,1024]{2,1,0:T(8,128)(2,1)}, u32[]{:S(2)}) copy-start(bf16[1,448,1024]{2,1,0:T(8,128)(2,1)} %param.11) | copy-start | bytes 2752516
  6.6 122.4 %all-gather.3.cloned.1.call-start = ((), (), s32[]{:S(2)}) async-start(), calls=%async_computation.4 | async-start | bytes 5898240 | tf_op jit(solution)/shard_map/all_gather | solution.py:58
  7.6 121.4 %copy-start.2 = (bf16[1,1024,448]{1,2,0:T(8,128)(2,1)S(1)}, bf16[1,1024,448]{1,2,0:T(8,128)(2,1)}, u32[]{:S(2)}) copy-start(bf16[1,1024,448]{1,2,0:T(8,128)(2,1)} %param.10) | copy-start | bytes 2752516
  65.3 72.4 %copy-start.3 = (bf16[1,1024,448]{1,2,0:T(8,128)(2,1)S(1)}, bf16[1,1024,448]{1,2,0:T(8,128)(2,1)}, u32[]{:S(2)}) copy-start(bf16[1,1024,448]{1,2,0:T(8,128)(2,1)} %param.9) | copy-start | bytes 2752516
  65.3 159.5 %reduce-scatter.2.cloned.1.call-start = ((), (), s32[]{:S(2)}) async-start(), calls=%async_computation.3 | async-start | bytes 5898240 | tf_op jit(solution)/shard_map/reduce_scatter | solution.py:66
  129.0 8.7 %copy-start.1 = (bf16[16,160,1024]{2,0,1:T(8,128)(2,1)S(1)}, bf16[16,160,1024]{2,0,1:T(8,128)(2,1)}, u32[]{:S(2)}) copy-start(bf16[16,160,1024]{2,0,1:T(8,128)(2,1)} %all-gather.3.cloned.1.call-done) | copy-start | bytes 15728644
  226.8 30.5 %all-to-all-start.1 = ((bf16[1,16,20,1024]{3,2,0,1:T(8,128)(2,1)}), bf16[1,16,20,1024]{3,2,0,1:T(8,128)(2,1)S(1)}, u32[]{:S(2)}, u32[]{:S(2)}) async-start(bf16[1,16,20,1024]{3,2,0,1:T(8,128)(2,1)} %bitcast.17), calls=%async_computation.2 | async-start | bytes 1572864 | tf_op jit(solution)/shard_map/all_to_all | solution.py:76
Sparse Core Ops, SparseCore 0:
  65.4 63.5 all-gather.2
  159.4 65.3 reduce-scatter.1
where the time goes:
time: 267 us
  waiting for transfers between devices  151 us (57%)
  blocking collectives  46.1 us (17%)
  local copies, waits for them, and re-layouts  20.2 us (8%)
  matrix products  19.7 us (7%)
  between operations  13.6 us (5%)
  starting transfers between devices  7.99 us (3%)
  other arithmetic  7.91 us (3%)
    reduce_scatter x1, waiting for transfers between devices, body(): lax.psum_scatter(product.astype(jnp.bfloat16).astype(jnp.float32).reshape...  65.5 us
    all_gather x1, waiting for transfers between devices, body(): lax.all_gather(arrived, 'tp', axis=2, tiled=True)  63.5 us
    all_to_all x1, blocking collectives, body(): lax.all_to_all(sending.reshape(experts, most, width), 'ep', split_axis=0,...  46.1 us
    all_to_all x1, waiting for transfers between devices, body(): lax.all_to_all(own_pieces, 'ep', split_axis=1, concat_axis=0, tiled=True)  22 us
    convert_element_type x1, local copies, waits for them, and re-layouts, body(): own_sums = lax.psum_scatter(product.astype(jnp.bfloat16).astype(jnp.float...  8.97 us
    dot_general x1, matrix products, expert_hidden(): jnp.einsum('e...d,edf->e...f', rows, up_weight, preferred_element_type=jn...  8.66 us
    all_to_all x1, starting transfers between devices, body(): lax.all_to_all(own_pieces, 'ep', split_axis=1, concat_axis=0, tiled=True)  7.74 us
    dot_general x1, matrix products, body(): jnp.einsum('tlnmf,lfd->tlnmd', by_source, down_weight, preferred_element_...  5.99 us
  transfers between devices with their start and end apart: 3, of which 3 were waited for; matrix products, arithmetic and copies ran while one was open for 0% of the time, Pallas kernels for 0%

commit v1 on v0

--- a/solution.py
+++ b/solution.py
@@ -54,9 +54,15 @@
         sending.reshape(experts, most, width), "ep", split_axis=0, concat_axis=1, tiled=True
     )
     arrived = arrived.reshape(local_experts, n_ep, most, width)
-    hidden = expert_hidden(
-        lax.all_gather(arrived, "tp", axis=2, tiled=True), gate_weight, up_weight
-    )
+
+    def order_lines(s0, axis_id, d_out):
+        e_next = jnp.concatenate(
+            lax.all_to_all(jnp.stack([s0 for _ in range(lax.axis_size(axis_id))]), axis_id, 0, 0),
+            axis=d_out,
+        )
+        return e_next
+
+    hidden = expert_hidden(order_lines(arrived, "tp", 2), gate_weight, up_weight)
     hidden = hidden.reshape(local_experts, n_ep * n_tp * most, inner)
     by_source = hidden.reshape(local_experts, n_ep, n_tp, most, inner).transpose(2, 0, 1, 3, 4)
     per_device = local_experts * n_ep * most

time: 267 us -> 321 us (1.20)
  blocking collectives: 46.1 us -> 168 us
  waiting for transfers between devices: 151 us -> 85.6 us
    all_to_all x0 -> x1, blocking collectives: none -> 122 us  [order_lines(): lax.all_to_all(jnp.stack([s0 for _ in range(lax.axis_size(axis_id))]), ax...]
    all_gather x1 -> x0, waiting for transfers between devices: 63.5 us -> none  [body(): lax.all_gather(arrived, 'tp', axis=2, tiled=True)]
  transfers between devices with their start and end apart: 3 -> 2, of which waited for: 3 -> 2; matrix products, arithmetic and copies ran while one was open for 0% -> 0% of each run, Pallas kernels for 0% -> 0%
where the time goes in v1:
time: 321 us; the launch traced here: 320 us
  blocking collectives  168 us (52%)
  waiting for transfers between devices  85.6 us (27%)
  local copies, waits for them, and re-layouts  20 us (6%)
  matrix products  17.8 us (6%)
  between operations  13.6 us (4%)
  other arithmetic  7.9 us (2%)
  starting transfers between devices  7.72 us (2%)
    all_to_all x1, blocking collectives, order_lines(): lax.all_to_all(jnp.stack([s0 for _ in range(lax.axis_size(axis_id))]), ax...  122 us
    reduce_scatter x1, waiting for transfers between devices, body(): lax.psum_scatter(product.astype(jnp.bfloat16).astype(jnp.float32).reshape...  63.6 us
    all_to_all x1, blocking collectives, body(): lax.all_to_all(sending.reshape(experts, most, width), 'ep', split_axis=0,...  46.1 us
    all_to_all x1, waiting for transfers between devices, body(): lax.all_to_all(own_pieces, 'ep', split_axis=1, concat_axis=0, tiled=True)  22 us
    convert_element_type x1, local copies, waits for them, and re-layouts, body(): own_sums = lax.psum_scatter(product.astype(jnp.bfloat16).astype(jnp.float...  8.97 us
    all_to_all x1, starting transfers between devices, body(): lax.all_to_all(own_pieces, 'ep', split_axis=1, concat_axis=0, tiled=True)  7.72 us
    dot_general x1, matrix products, expert_hidden(): jnp.einsum('e...d,edf->e...f', rows, up_weight, preferred_element_type=jn...  6.54 us
  transfers between devices with their start and end apart: 2, of which 2 were waited for; matrix products, arithmetic and copies ran while one was open for 0% of the time, Pallas kernels for 0%

profile of v1, /device:TPU:513, one launch (start us, length us, event | category | flops | bytes accessed | tf_op | source)
XLA Modules:
  0.0 320.3 jit_solution(4035641382084505895)
XLA Ops:
  6.5 0.0 copy-start
  6.6 0.0 reduce-scatter.2.cloned.1.call-start
  6.6 1.0 copy.21
  7.6 0.3 eq.26
  7.9 0.3 reshape.117
  8.2 4.6 %reduce-window.6 = s32[8,16,2,128]{3,1,2,0:T(8,128)S(1)} reduce-window(s32[8,16,2,128]{3,1,2,0:T(8,128)S(1)} %fusion.22, s32[]{:T(128)} %constant.6.clone.1), window={size=1x1x1x128 pad=0_0x0_0x0_0x127_0}, to_apply=%region_0.0 | reduce-window | flops 4161536 | bytes 262148 | tf_op jit(solution)/shard_map/reduce-window
  12.7 0.1 slice.26
  12.8 0.2 copy.23
  13.0 0.1 fusion.23
  13.1 1.1 fusion.10
  14.2 1.1 fusion.12
  15.3 0.3 broadcast_in_dim.5
  15.5 0.2 reshape.142
  15.7 0.1 fusion.21
  15.9 1.9 scatter_custom_fusion
  17.7 0.1 reshape.120
  17.9 46.1 %all_to_all.23 = bf16[16,20,1024]{2,1,0:T(8,128)(2,1)S(1)} all-to-all(bf16[16,20,1024]{2,1,0:T(8,128)(2,1)S(1)} %reshape.120), channel_id=1, replica_groups=mesh['grp'=2,'ep'=16,'tp'=8] {'ep'}, dimensions={0} | all-to-all | bytes 1310720 | tf_op jit(solution)/shard_map/all_to_all | solution.py:53
  64.0 0.4 copy.26
  64.3 0.7 stack.3
  65.0 0.0 copy-start.1
  65.0 121.6 %all_to_all.24 = bf16[8,1,16,20,1024]{4,2,3,1,0:T(8,128)(2,1)S(1)} all-to-all(bf16[8,1,16,20,1024]{4,2,3,1,0:T(8,128)(2,1)S(1)} %stack.3), channel_id=1, replica_groups=mesh['grp'=2,'ep'=16,'tp'=8] {'tp'}, dimensions={0} | all-to-all | bytes 10485760 | tf_op jit(solution)/shard_map/all_to_all | solution.py:60
  186.6 0.0 copy-done.1
  186.6 0.0 copy-start.2
  186.6 6.5 %fusion = f32[16,160,448]{2,1,0:T(8,128)S(1)} fusion(bf16[16,160,1024]{2,0,1:T(8,128)(2,1)S(1)} %bitcast.79, bf16[1,1024,448]{1,2,0:T(8,128)(2,1)S(1)} %copy-done.1), kind=kOutput, calls=%fused_computation.4 | convolution fusion | flops 2348810240 | bytes 10747904 | tf_op jit(solution)/shard_map/e...d,edf->e...f/dot_general | solution.py:17
  193.2 0.0 copy-done.2
  193.2 5.0 %multiply_convert_fusion = bf16[16,160,448]{2,1,0:T(8,128)(2,1)S(1)} fusion(f32[16,160,448]{2,1,0:T(8,128)S(1)} %fusion, bf16[16,160,1024]{2,0,1:T(8,128)(2,1)S(1)} %bitcast.80, bf16[1,1024,448]{1,2,0:T(8,128)(2,1)S(1)} %copy-done.2), kind=kOutput, calls=%fused_computation.3 | convolution fusion | flops 2355691520 | bytes 13041664 | tf_op jit(solution)/shard_map/e...d,edf->e...f/dot_general | solution.py:16
  198.2 1.5 copy.30
  199.7 0.0 copy-done
  199.7 6.2 %convert_bitcast_fusion = bf16[8,1,16,20,1024]{4,3,2,0,1:T(8,128)(2,1)} fusion(bf16[8,16,20,448]{3,1,2,0:T(8,128)(2,1)S(1)} %bitcast.81, bf16[1,448,1024]{2,1,0:T(8,128)(2,1)S(1)} %copy-done), kind=kOutput, calls=%fused_computation.2 | convolution fusion | flops 2351431680 | bytes 8454144 | tf_op jit(solution)/shard_map/tlnmf,lfd->tlnmd/dot_general | solution.py:69
  205.9 9.0 %convert_element_type.51 = bf16[2560,1024]{1,0:T(8,128)(2,1)} reshape(bf16[8,1,16,20,1024]{4,3,2,0,1:T(8,128)(2,1)} %convert_bitcast_fusion) | data formatting | bytes 10485760 | tf_op jit(solution)/shard_map/convert_element_type | solution.py:76
  214.9 0.1 reduce-scatter.2.cloned.1.call-update
  214.9 63.6 %reduce-scatter.2.cloned.1.call-done = bf16[320,1024]{1,0:T(8,128)(2,1)} async-done(((bf16[2560,1024]{1,0:T(8,128)(2,1)}), bf16[320,1024]{1,0:T(8,128)(2,1)}) %reduce-scatter.2.cloned.1.call-update) | async-done | bytes 655376 | tf_op jit(solution)/shard_map/reduce_scatter | solution.py:72
  278.5 2.0 reshape.127
  280.5 7.7 %all-to-all-start.2 = ((bf16[1,16,20,1024]{3,2,0,1:T(8,128)(2,1)}), bf16[1,16,20,1024]{3,2,0,1:T(8,128)(2,1)S(1)}, u32[]{:S(2)}, u32[]{:S(2)}) async-start(bf16[1,16,20,1024]{3,2,0,1:T(8,128)(2,1)} %bitcast.22), calls=%async_computation.3 | async-start | bytes 1572864 | tf_op jit(solution)/shard_map/all_to_all | solution.py:82
  288.2 0.7 constant_dynamic-slice_fusion
  288.9 22.0 %all-to-all-done.2 = bf16[1,16,20,1024]{3,2,0,1:T(8,128)(2,1)S(1)} async-done(((bf16[1,16,20,1024]{3,2,0,1:T(8,128)(2,1)}), bf16[1,16,20,1024]{3,2,0,1:T(8,128)(2,1)S(1)}, u32[]{:S(2)}, u32[]{:S(2)}) %all-to-all-start.2) | async-done | bytes 655392 | tf_op jit(solution)/shard_map/all_to_all | solution.py:82
  311.0 0.1 reshape.128
  311.1 1.2 gather_fusion
  312.3 0.2 reshape.129
  312.5 0.1 copy_convert_fusion
  312.6 0.8 fusion.15
  (7 shorter events, 0.1 us)
Async XLA Ops:
  6.5 193.1 %copy-start = (bf16[1,448,1024]{2,1,0:T(8,128)(2,1)S(1)}, bf16[1,448,1024]{2,1,0:T(8,128)(2,1)}, u32[]{:S(2)}) copy-start(bf16[1,448,1024]{2,1,0:T(8,128)(2,1)} %param.11) | copy-start | bytes 2752516
  6.6 272.0 %reduce-scatter.2.cloned.1.call-start = ((), (), s32[]{:S(2)}) async-start(), calls=%async_computation.4 | async-start | bytes 5898240 | tf_op jit(solution)/shard_map/reduce_scatter | solution.py:72
  65.0 121.6 %copy-start.1 = (bf16[1,1024,448]{1,2,0:T(8,128)(2,1)S(1)}, bf16[1,1024,448]{1,2,0:T(8,128)(2,1)}, u32[]{:S(2)}) copy-start(bf16[1,1024,448]{1,2,0:T(8,128)(2,1)} %param.10) | copy-start | bytes 2752516
  186.6 6.5 %copy-start.2 = (bf16[1,1024,448]{1,2,0:T(8,128)(2,1)S(1)}, bf16[1,1024,448]{1,2,0:T(8,128)(2,1)}, u32[]{:S(2)}) copy-start(bf16[1,1024,448]{1,2,0:T(8,128)(2,1)} %param.9) | copy-start | bytes 2752516
  280.5 30.4 %all-to-all-start.2 = ((bf16[1,16,20,1024]{3,2,0,1:T(8,128)(2,1)}), bf16[1,16,20,1024]{3,2,0,1:T(8,128)(2,1)S(1)}, u32[]{:S(2)}, u32[]{:S(2)}) async-start(bf16[1,16,20,1024]{3,2,0,1:T(8,128)(2,1)} %bitcast.22), calls=%async_computation.3 | async-start | bytes 1572864 | tf_op jit(solution)/shard_map/all_to_all | solution.py:82
Sparse Core Ops, SparseCore 0:
  215.1 63.3 reduce-scatter.1
